TPU v7x, 32 devices: a whole 2x2x4 slice. The times are simulated.
32 devices in a mesh: sp: 8 (over z, x), tp: 4 (over y, core).
Axes of the slice: x: 2, y: 2, z: 4, core: 2. Of those that a mesh axis runs over, the one named last changes fastest.
Arguments:
- mixer_out: bfloat16 [1024, 2048], P('sp'), may hold values from -6 to 6
- out_grad: bfloat16 [1024, 2048], P('sp'), may hold values from -2 to 2
- route_ids: int32 [1024, 2], P('sp'), may hold values from 0 to 7, all different within a row; in each aligned block of 128 rows (0 to 127, 128 to 255, ...) at most 64 rows name the same one
- route_weights: float32 [1024, 2], P('sp'), may hold values from 0.2 to 1.2
- gate_branch: bfloat16 [1024, 2048], P('sp', 'tp'), may hold values from -4 to 4
- states: float32 [1024, 2048], P('sp', 'tp'), may hold values from -6 to 6
- decay: float32 [1024, 2048], P('sp', 'tp'), may hold values from 0 to 1
- w_proj: bfloat16 [2048, 2048], P(None, 'tp'), may hold values from -0.125 to 0.125
- w_gate: bfloat16 [8, 2048, 2048], P('sp', 'tp'), may hold values from -0.125 to 0.125
- w_up: bfloat16 [8, 2048, 2048], P('sp', 'tp'), may hold values from -0.125 to 0.125
- w_down: bfloat16 [8, 2048, 2048], P('sp', 'tp'), may hold values from -0.125 to 0.125
Outputs:
- grad_w_gate: bfloat16 [8, 2048, 2048], P('sp', 'tp')
- grad_w_up: bfloat16 [8, 2048, 2048], P('sp', 'tp')
- grad_w_down: bfloat16 [8, 2048, 2048], P('sp', 'tp')
- grad_w_proj: float32 [2048, 2048], P('sp', 'tp')
- grad_branch: bfloat16 [1024, 2048], P('sp', 'tp')
- grad_drive: float32 [1024, 2048], P('sp', 'tp')
- grad_decay: float32 [1024, 2048], P('sp', 'tp')
Inputs may be any that keep to these rules, and one draw needn't show every extreme that they name: `route_ids`: each row names 2 different experts. In the rows of one index of sp no expert is named more than 64 times, a bound that some block reaches.
All inputs are finite; a program needn't handle non-finite values.
Results may differ from a plain program's by a relative error of at most 0.02.
Values may be sent and summed in bfloat16 or wider, within the bound.
A program may use at most 64 MiB of HBM per device.

v0:
```python
import functools

import jax
import jax.numpy as jnp
from jax import lax
from jax.experimental import pallas as pl
from jax.experimental.pallas import tpu as pltpu
from jax.sharding import PartitionSpec as P

MESH = pl.DeviceIdType.MESH
F32 = jnp.float32
BF16 = jnp.bfloat16
CHUNKS = 2


def dot(a, b, ca, cb):
    return lax.dot_general(a, b, (((ca,), (cb,)), ((), ())), preferred_element_type=F32)


def kernel(
    n_sp,
    n_tp,
    ids,
    wts,
    mix,
    og,
    gb,
    st,
    dc,
    wp_h,
    wg_h,
    wu_h,
    wd_h,
    dwg_h,
    dwu_h,
    dwd_h,
    gproj,
    gbr,
    gdr,
    gdc,
    wp,
    wg,
    wu,
    wd,
    dwg,
    dwu,
    dwd,
    sel,
    sw,
    send,
    xc,
    ga,
    pv,
    gg,
    ug,
    hid,
    pb,
    po,
    rc,
    qb,
    ry,
    fb,
    ret,
    mt,
    mr,
    cs,
    cr,
    w_sem,
    o_sem,
    l_sem,
    sp_s,
    sp_r,
    core_s,
    core_r,
    y_s,
    y_r,
    ga_s,
    ga_r,
    pv_sem,
    pc_s,
    pc_r,
    py_s,
    py_r,
    ret_s,
    ret_r,
    mtc_s,
    mtc_r,
    mty_s,
    mty_r,
    mr_s,
    mr_r,
    mrc_s,
    mrc_r,
    c_s,
    c_r,
):
    i = lax.axis_index("sp")
    t = lax.axis_index("tp")
    ny = n_tp // 2
    y, c = t // 2, t % 2
    tok = mix.shape[0]
    cap = xc.shape[3]
    dg = xc.shape[4]
    half = n_sp // CHUNKS
    rows = half * cap
    slots = n_sp * cap
    peer = (i, y * 2 + 1 - c)
    straight = ()

    def columns(g):
        return pl.ds(pl.multiple_of(g * dg, dg), dg)

    def later(k):
        return lax.rem(i + k, n_sp)

    def before(k):
        return lax.rem(i + n_sp - k, n_sp)

    def y_up(q):
        return lax.rem(y + q, ny)

    def remote(src, dst, s, r, who):
        return pltpu.make_async_remote_copy(
            src_ref=src, dst_ref=dst, send_sem=s, recv_sem=r, device_id=who, device_id_type=MESH
        )

    loads = [
        pltpu.make_async_copy(a, b, w_sem.at[n])
        for n, (a, b) in enumerate(((wg_h, wg), (wu_h, wu), (wd_h, wd), (wp_h, wp)))
    ]
    for load in loads:
        load.start()

    barrier = pltpu.get_barrier_semaphore()
    for k in range(1, n_sp):
        pl.semaphore_signal(barrier, inc=1, device_id=(later(k), t), device_id_type=MESH)
    for k in range(1, n_tp):
        pl.semaphore_signal(
            barrier, inc=1, device_id=(i, lax.rem(t + k, n_tp)), device_id_type=MESH
        )

    experts_iota = lax.broadcasted_iota(jnp.int32, (n_sp, tok), 0)
    named = jnp.zeros((n_sp, tok), F32)
    weight = jnp.zeros((n_sp, tok), F32)
    for k in range(ids.shape[0]):
        hit = ids[k : k + 1, :] == experts_iota
        named = jnp.where(hit, 1.0, named)
        weight = jnp.where(hit, wts[k : k + 1, :], weight)
    earlier = (
        lax.broadcasted_iota(jnp.int32, (tok, tok), 0)
        < lax.broadcasted_iota(jnp.int32, (tok, tok), 1)
    )
    place = dot(named.astype(BF16), jnp.where(earlier, 1.0, 0.0).astype(BF16), 1, 0)
    place = jnp.where(named > 0.5, place, -1.0).astype(jnp.int32)
    slot_iota = lax.broadcasted_iota(jnp.int32, (cap, tok), 0)
    for e in range(n_sp):
        here = jnp.where(place[e : e + 1, :] == slot_iota, 1.0, 0.0)
        slot_weight = jnp.sum(here * weight[e : e + 1, :], axis=1, keepdims=True)
        sel[e * cap : (e + 1) * cap, :] = here.astype(BF16)
        sw[e * cap : (e + 1) * cap, :] = jnp.broadcast_to(slot_weight, (cap, sw.shape[1]))
    chosen = sel[...]
    for q in range(ny):
        cols = columns(2 * y_up(q) + c)
        send[0, q] = dot(chosen, mix[:, cols], 1, 0).astype(BF16).reshape(n_sp, cap, dg)
        send[1, q] = (
            (dot(chosen, og[:, cols], 1, 0) * sw[:, 0:1]).astype(BF16).reshape(n_sp, cap, dg)
        )
    pl.semaphore_wait(barrier, n_sp + n_tp - 2)

    pending = []

    def go(copy):
        copy.start()
        pending.append(copy)

    def groups(k):
        return range(ny) if k in straight else range(1)

    def dispatch(q, k):
        return remote(
            send.at[:, q, later(k)],
            xc.at[:, 2 * y_up(q) + c, i],
            sp_s.at[q, k],
            sp_r.at[q, k],
            (later(k), t),
        )

    for k in range(1, n_sp):
        for q in groups(k):
            go(dispatch(q, k))
    go(
        remote(
            st.at[pl.ds(tok - 8, 8)], pv, pv_sem.at[0], pv_sem.at[1], (later(1), t)
        )
    )
    pv_copy = pending[-1]

    mine = pl.ds(pl.multiple_of(i * cap, cap), cap)
    here, slot_weight = sel[mine, :], sw[mine, 0:1]
    for g in range(n_tp):
        cols = slice(g * dg, (g + 1) * dg)
        xc[0, g, i] = dot(here, mix[:, cols], 1, 0).astype(BF16)
        xc[1, g, i] = (dot(here, og[:, cols], 1, 0) * slot_weight).astype(BF16)
    ga[i] = (gb[...].astype(F32) * st[...]).astype(BF16)

    def to_core(q, k):
        block = xc.at[:, 2 * y_up(q) + c, before(k)]
        return remote(block, block, core_s.at[q, k], core_r.at[q, k], peer)

    def to_y(q, k):
        block = xc.at[:, t, before(k)]
        return remote(
            block, block, y_s.at[q, k], y_r.at[q, k], (i, 2 * y_up(q) + c)
        )

    def from_y(q, k):
        block = xc.at[:, 2 * y_up(ny - q) + c, before(k)]
        return remote(block, block, y_s.at[q, k], y_r.at[q, k], (i, 2 * y_up(q) + c))

    def from_sp(q, k):
        return remote(
            send.at[:, q, later(k)],
            xc.at[:, 2 * y_up(q) + c, before(k)],
            sp_s.at[q, k],
            sp_r.at[q, k],
            (later(k), t),
        )

    def from_core(q, k):
        block = xc.at[:, 2 * y_up(q) + 1 - c, before(k)]
        return remote(block, block, core_s.at[q, k], core_r.at[q, k], peer)

    def spread(k):
        for q in groups(k):
            from_sp(q, k).wait_recv()
        if k not in straight:
            for q in range(1, ny):
                go(to_y(q, k))
        for q in groups(k):
            go(to_core(q, k))

    def hand_on(k):
        if k in straight:
            return
        for q in range(1, ny):
            from_y(q, k).wait_recv()
            go(to_core(ny - q, k))

    def expert(m):
        order = [before(m * half + q) for q in range(half)]

        def rows_of(which, g):
            return jnp.concatenate([xc[which, g, s] for s in order], axis=0)

        gate = up = hg = None
        for g in range(n_tp):
            cols = slice(g * dg, (g + 1) * dg)
            x, cot = rows_of(0, g), rows_of(1, g)
            parts = (dot(x, wg[:, cols], 1, 1), dot(x, wu[:, cols], 1, 1), dot(cot, wd[:, cols], 1, 1))
            if g == 0:
                gate, up, hg = parts
            else:
                gate, up, hg = gate + parts[0], up + parts[1], hg + parts[2]
        s = jax.nn.sigmoid(gate)
        silu = gate * s
        hidden = (silu * up).astype(BF16)
        up_grad = (hg * silu).astype(BF16)
        gate_grad = (hg * up * s * (1.0 + gate * (1.0 - s))).astype(BF16)
        for q, src in enumerate(order):
            part = slice(q * cap, (q + 1) * cap)
            hid[src] = hidden[part]
            ug[src] = up_grad[part]
            gg[src] = gate_grad[part]
        return gate_grad, up_grad

    def partial(gate_grad, up_grad, g):
        cols = columns(g)
        return (dot(gate_grad, wg[:, cols], 1, 0) + dot(up_grad, wu[:, cols], 1, 0)).astype(BF16)

    def swap_core(m, q):
        return remote(pb.at[m, q], rc.at[m, q], pc_s.at[m, q], pc_r.at[m, q], peer)

    def swap_y(m, q):
        return remote(
            qb.at[m, q], ry.at[m, q], py_s.at[m, q], py_r.at[m, q], (i, 2 * y_up(q) + c)
        )

    def partials(m, grads):
        for q in list(range(1, ny)) + [0]:
            pb[m, q] = partial(*grads, 2 * y_up(q) + 1 - c)
            go(swap_core(m, q))
        for q in list(range(1, ny)) + [0]:
            po[m, q] = partial(*grads, 2 * y_up(q) + c)

    def fold_core(m):
        for q in range(1, ny):
            swap_core(m, q).wait_recv()
            qb[m, q] = (po[m, q].astype(F32) + rc[m, q].astype(F32)).astype(BF16)
            go(swap_y(m, q))

    def home(k):
        m, q = k // half, k % half
        return remote(
            fb.at[m, pl.ds(q * cap, cap)], ret.at[i], ret_s.at[k], ret_r.at[k], (before(k), t)
        )

    def fold_y(m):
        swap_core(m, 0).wait_recv()
        total = po[m, 0].astype(F32) + rc[m, 0].astype(F32)
        for q in range(1, ny):
            swap_y(m, q).wait_recv()
            total = total + ry[m, q].astype(F32)
        fb[m] = total.astype(BF16)
        for q in range(half):
            k = m * half + q
            if k == 0:
                pltpu.make_async_copy(
                    fb.at[0, pl.ds(0, cap)], ret.at[i], l_sem.at[1]
                ).start()
            else:
                go(home(k))

    def weight_grad(left, which, out, out_h, n):
        a = left[...].reshape(slots, left.shape[2])
        for g in range(n_tp):
            b = xc[which, g].reshape(slots, dg)
            out[:, g * dg : (g + 1) * dg] = dot(a, b, 0, 0).astype(BF16)
        copy = pltpu.make_async_copy(out, out_h, o_sem.at[n])
        copy.start()
        return copy

    for k in range(1, n_sp):
        spread(k)
        if 1 < k <= half:
            hand_on(k - 1)

    pair_peer = (i + 1 - 2 * (i % 2), t)

    def share_gated(k):
        return remote(ga.at[i], ga.at[i], ga_s.at[k], ga_r.at[k], (later(k), t))

    def get_gated(k):
        return remote(ga.at[i], ga.at[before(k)], ga_s.at[k], ga_r.at[k], (later(k), t))

    def pass_gated(k):
        block = ga.at[before(k)]
        return remote(block, block, ga_s.at[k + 1], ga_r.at[k + 1], pair_peer)

    def passed_gated(k):
        block = ga.at[lax.rem(pair_peer[0] + n_sp - k, n_sp)]
        return remote(block, block, ga_s.at[k + 1], ga_r.at[k + 1], pair_peer)

    for k in range(2, n_sp, 2):
        go(share_gated(k))
    for load in loads:
        load.wait()

    def arrived(m):
        for k in range(max(1, m * half), (m + 1) * half):
            for q in range(ny):
                from_core(q, k).wait_recv()

    arrived(0)
    grads = expert(0)
    for k in range(half, n_sp):
        hand_on(k)
    partials(0, grads)
    arrived(1)
    grads = expert(1)
    fold_core(0)
    partials(1, grads)
    outs = [weight_grad(gg, 0, dwg, dwg_h, 0)]
    fold_core(1)
    fold_y(0)
    outs.append(weight_grad(ug, 0, dwu, dwu_h, 1))
    fold_y(1)
    outs.append(weight_grad(hid, 1, dwd, dwd_h, 2))
    for k in range(0, n_sp, 2):
        if k:
            get_gated(k).wait_recv()
        go(pass_gated(k))

    pltpu.make_async_copy(fb.at[0, pl.ds(0, cap)], ret.at[i], l_sem.at[1]).wait()

    def from_expert(k):
        m, q = k // half, k % half
        return remote(
            fb.at[m, pl.ds(q * cap, cap)],
            ret.at[later(k)],
            ret_s.at[k],
            ret_r.at[k],
            (before(k), t),
        )

    for k in range(1, n_sp):
        from_expert(k).wait_recv()
    routed = dot(ret[...].reshape(slots, dg), sel[...], 0, 0)
    mid = (og[:, columns(t)].astype(F32).T + routed).astype(BF16)
    mt[t] = mid

    def mid_core(q):
        block = mt.at[2 * y_up(q) + c]
        return remote(block, block, mtc_s.at[q], mtc_r.at[q], peer)

    def mid_from_core(q):
        block = mt.at[2 * y_up(q) + 1 - c]
        return remote(block, block, mtc_s.at[q], mtc_r.at[q], peer)

    def mid_y(q):
        return remote(mt.at[t], mt.at[t], mty_s.at[q], mty_r.at[q], (i, 2 * y_up(q) + c))

    def mid_from_y(q):
        block = mt.at[2 * y_up(ny - q) + c]
        return remote(block, block, mty_s.at[q], mty_r.at[q], (i, 2 * y_up(q) + c))

    for q in range(1, ny):
        go(mid_y(q))
    go(mid_core(0))

    row = lax.broadcasted_iota(jnp.int32, dc.shape, 0)
    decay = dc[...]
    head = decay[0:1, :]
    factor = jnp.where(row < tok - 1, pltpu.roll(decay, tok - 1, 0), 1.0)
    for q in range(1, ny):
        mid_from_y(q).wait_recv()
        go(mid_core(ny - q))
    for q in range(ny):
        mid_from_core(q).wait_recv()

    share = 2 * mr.shape[2]
    per = dg // share if dg >= share else 1

    part = share // 2

    def rows_for(s, h):
        first = (s % per) * share + h * part
        return mt.at[s // per, pl.ds(pl.multiple_of(first, part), part)]

    def share_rows(k):
        return remote(rows_for(later(k), c), mr.at[i, c], mr_s.at[k], mr_r.at[k], (later(k), t))

    def get_rows(k):
        return remote(
            rows_for(later(k), c), mr.at[before(k), c], mr_s.at[k], mr_r.at[k], (later(k), t)
        )

    def swap_rows(k, h):
        block = mr.at[before(k), h]
        return remote(block, block, mrc_s.at[k], mrc_r.at[k], peer)

    for k in range(1, n_sp):
        go(share_rows(k))
    for h in range(2):
        own_rows = pltpu.make_async_copy(rows_for(i, h), mr.at[i, h], l_sem.at[h])
        own_rows.start()
        own_rows.wait()

    act = dot(mt[...].reshape(n_tp * dg, tok), wp[...], 0, 0)
    grad = act * gb[...].astype(F32)
    gbr[...] = (act * st[...]).astype(BF16)
    step = 1
    while step < tok:
        inside = row < tok - step
        grad = grad + jnp.where(inside, factor * pltpu.roll(grad, tok - step, 0), 0.0)
        factor = factor * jnp.where(inside, pltpu.roll(factor, tok - step, 0), 1.0)
        step *= 2
    pair = jnp.concatenate([head * factor[0:1, :], head * grad[0:1, :]], axis=0)
    pair = jnp.concatenate([pair, jnp.zeros((6, pair.shape[1]), F32)], axis=0)
    cs[...] = pair
    cr[i] = pair

    def share_carry(k):
        return remote(cs, cr.at[i], c_s.at[k], c_r.at[k], (later(k), t))

    def get_carry(k):
        return remote(cs, cr.at[before(k)], c_s.at[k], c_r.at[k], (later(k), t))

    for k in range(1, n_sp):
        go(share_carry(k))

    for k in range(1, n_sp):
        get_rows(k).wait_recv()
        go(swap_rows(k, c))
    for k in range(0, n_sp, 2):
        passed_gated(k).wait_recv()
    total = None
    for k in range(n_sp):
        if k:
            swap_rows(k, 1 - c).wait_recv()
        src = before(k)
        term = dot(mr[src].reshape(share, tok), ga[src], 1, 0)
        total = term if total is None else total + term
    gproj[...] = total

    for k in range(1, n_sp):
        get_carry(k).wait_recv()
    carry = jnp.zeros((1, pair.shape[1]), F32)
    for s in range(n_sp - 1, 0, -1):
        carry = jnp.where(s > i, cr[s, 1:2, :] + cr[s, 0:1, :] * carry, carry)
    drive = grad + factor * carry
    gdr[...] = drive
    pv_copy.wait_recv()
    states = st[...]
    last = jnp.where(i > 0, pv[7:8, :], 0.0)
    previous = jnp.where(row == 0, last, pltpu.roll(states, 1, 0))
    gdc[...] = drive * previous

    for copy in outs:
        copy.wait()
    for copy in pending:
        copy.wait_send()


def settle(count, *refs):
    ins, outs, held = refs[:count], refs[count : 2 * count], refs[2 * count : 3 * count]
    in_sem, out_sem = refs[3 * count :]
    jobs = []
    for n in range(count):
        pieces = 2 if n < 3 else 1
        rows = ins[n].shape[0] // pieces
        for p in range(pieces):
            part = pl.ds(p * rows, rows)
            jobs.append(
                (
                    pltpu.make_async_copy(ins[n].at[part], held[n].at[part], in_sem.at[n, p]),
                    pltpu.make_async_copy(held[n].at[part], outs[n].at[part], out_sem.at[n, p]),
                )
            )
    for bring, _ in jobs:
        bring.start()
    for bring, put in jobs:
        bring.wait()
        put.start()
    for _, put in jobs:
        put.wait()


def local(
    mixer_out,
    out_grad,
    route_ids,
    route_weights,
    gate_branch,
    states,
    decay,
    w_proj,
    w_gate,
    w_up,
    w_down,
):
    tok, width = mixer_out.shape
    top = route_ids.shape[1]
    n_sp, n_tp = lax.axis_size("sp"), lax.axis_size("tp")
    ny = n_tp // 2
    assert w_gate.shape[0] == 1
    cap = 2 * top * tok // n_sp
    dg = width // n_tp
    hidden = w_gate.shape[1]
    channels = states.shape[1]
    half_rows = n_sp * cap // CHUNKS
    share = width // n_sp
    vmem = pl.BlockSpec(memory_space=pltpu.VMEM)
    hbm = pl.BlockSpec(memory_space=pl.ANY)
    dma = pltpu.SemaphoreType.DMA
    weight = (hidden, width)
    outs = pl.pallas_call(
        functools.partial(kernel, n_sp, n_tp),
        out_shape=[jax.ShapeDtypeStruct(weight, BF16)] * 3
        + [
            jax.ShapeDtypeStruct((share, channels), F32),
            jax.ShapeDtypeStruct((tok, channels), BF16),
            jax.ShapeDtypeStruct((tok, channels), F32),
            jax.ShapeDtypeStruct((tok, channels), F32),
        ],
        in_specs=[vmem] * 7 + [hbm] * 4,
        out_specs=[hbm] * 3 + [vmem] * 4,
        scratch_shapes=[
            pltpu.VMEM((width, channels), BF16),
            *([pltpu.VMEM(weight, BF16)] * 6),
            pltpu.VMEM((n_sp * cap, tok), BF16),
            pltpu.VMEM((n_sp * cap, 128), F32),
            pltpu.VMEM((2, ny, n_sp, cap, dg), BF16),
            pltpu.VMEM((2, n_tp, n_sp, cap, dg), BF16),
            pltpu.VMEM((n_sp, tok, channels), BF16),
            pltpu.VMEM((8, channels), F32),
            *([pltpu.VMEM((n_sp, cap, hidden), BF16)] * 3),
            *([pltpu.VMEM((CHUNKS, ny, half_rows, dg), BF16)] * 5),
            pltpu.VMEM((CHUNKS, half_rows, dg), BF16),
            pltpu.VMEM((n_sp, cap, dg), BF16),
            pltpu.VMEM((n_tp, dg, tok), BF16),
            pltpu.VMEM((n_sp, 2, share // 2, tok), BF16),
            pltpu.VMEM((8, channels), F32),
            pltpu.VMEM((n_sp, 8, channels), F32),
            dma((4,)),
            dma((3,)),
            dma((3,)),
            *([dma((ny, n_sp))] * 6),
            dma((n_sp,)),
            dma((n_sp,)),
            dma((2,)),
            *([dma((CHUNKS, ny))] * 4),
            dma((n_sp,)),
            dma((n_sp,)),
            *([dma((ny,))] * 4),
            *([dma((n_sp,))] * 6),
        ],
        compiler_params=pltpu.CompilerParams(
            collective_id=0, has_side_effects=True, vmem_limit_bytes=60 * 1024 * 1024
        ),
    )(
        route_ids.T,
        route_weights.T,
        mixer_out,
        out_grad,
        gate_branch,
        states,
        decay,
        w_proj,
        w_gate[0],
        w_up[0],
        w_down[0],
    )
    count = len(outs)
    outs = pl.pallas_call(
        functools.partial(settle, count),
        out_shape=[jax.ShapeDtypeStruct(o.shape, o.dtype) for o in outs],
        in_specs=[hbm] * count,
        out_specs=[hbm] * count,
        scratch_shapes=[
            *(pltpu.VMEM(o.shape, o.dtype) for o in outs),
            dma((count, 2)),
            dma((count, 2)),
        ],
    )(*outs)
    return (outs[0][None], outs[1][None], outs[2][None], *outs[3:])


def solution(mesh):
    placed = (
        P("sp", None),
        P("sp", None),
        P("sp", None),
        P("sp", None),
        P("sp", "tp"),
        P("sp", "tp"),
        P("sp", "tp"),
        P(None, "tp"),
        P("sp", "tp", None),
        P("sp", "tp", None),
        P("sp", "tp", None),
    )
    return jax.shard_map(
        local,
        mesh=mesh,
        in_specs=placed,
        out_specs=(
            P("sp", "tp", None),
            P("sp", "tp", None),
            P("sp", "tp", None),
            P("sp", "tp"),
            P("sp", "tp"),
            P("sp", "tp"),
            P("sp", "tp"),
        ),
        check_vma=False,
    )
```

profile of v0, /device:TPU:0, one launch (start us, length us, event | category | flops | bytes accessed | tf_op | source)
XLA Modules:
  0.0 91.3 jit_solution(13950462829740153176)
XLA Ops:
  0.6 84.6 %shard_map.162 = (bf16[512,2048]{1,0:T(8,128)(2,1)}, bf16[512,2048]{1,0:T(8,128)(2,1)}, bf16[512,2048]{1,0:T(8,128)(2,1)}, f32[256,512]{1,0:T(8,128)}, bf16[128,...) custom-call(s32[2,128]{1,0:T(2,128)} %bitcast.11, f32[2,128]{1,0:T(2,128)} %bitcast.12, ...), custom_call_target="tpu_custom_call" | custom-call | tf_op jit(solution)/shard_map/pallas_call | solution.py:566
  85.2 6.0 %shard_map.163 = (bf16[512,2048]{1,0:T(8,128)(2,1)}, bf16[512,2048]{1,0:T(8,128)(2,1)}, bf16[512,2048]{1,0:T(8,128)(2,1)}, f32[256,512]{1,0:T(8,128)}, bf16[128,...) custom-call(bf16[512,2048]{1,0:T(8,128)(2,1)} %get-tuple-element.21.refs_0_, ...), custom_call_target="tpu_custom_call" | custom-call | tf_op jit(solution)/shard_map/pallas_call | solution.py:624
where the time goes:
time: 91.7 us; the launch traced here: 91.3 us
  Pallas kernels  90.6 us (99%)
    pallas_call x1, Pallas kernels, local(): pl.pallas_call(functools.partial(kernel, n_sp, n_tp), out_shape=[jax.Shap...  84.6 us
    pallas_call x1, Pallas kernels, local(): pl.pallas_call(functools.partial(settle, count), out_shape=[jax.ShapeDtyp...  6.03 us

commit v1 on v0

v1 whole, which is shorter than its diff:
```python
import functools

import jax
import jax.numpy as jnp
from jax import lax
from jax.experimental import pallas as pl
from jax.experimental.pallas import tpu as pltpu
from jax.sharding import PartitionSpec as P

MESH = pl.DeviceIdType.MESH
F32 = jnp.float32
BF16 = jnp.bfloat16
LIMIT = 44 * 1024 * 1024


def dot(a, b, ca, cb):
    return lax.dot_general(a, b, (((ca,), (cb,)), ((), ())), preferred_element_type=F32)


def kernel(
    n_sp,
    n_tp,
    ids_h,
    wts_h,
    mix_h,
    og_h,
    gb_h,
    st_h,
    dc_h,
    wp_h,
    wg_h,
    wu_h,
    wd_h,
    dwg,
    dwu,
    dwd,
    gproj,
    gbr,
    gdr,
    gdc,
    ids,
    wts,
    mix,
    og,
    gb,
    st,
    dc,
    wp,
    wg,
    wu,
    wd,
    sel,
    sw,
    send,
    xc,
    ga,
    pv,
    gg,
    ug,
    hid,
    pb,
    po,
    rc,
    qb,
    ry,
    fb,
    ret,
    mt,
    mr,
    cs,
    cr,
    w_sem,
    sp_s,
    sp_r,
    core_s,
    core_r,
    y_s,
    y_r,
    ga_s,
    ga_r,
    pv_sem,
    pc_s,
    pc_r,
    py_s,
    py_r,
    ret_s,
    ret_r,
    mtc_s,
    mtc_r,
    mty_s,
    mty_r,
    mr_s,
    mr_r,
    mrc_s,
    mrc_r,
    c_s,
    c_r,
):
    i = lax.axis_index("sp")
    t = lax.axis_index("tp")
    ny = n_tp // 2
    y, c = t // 2, t % 2
    tok = mix.shape[0]
    cap = xc.shape[3]
    dg = xc.shape[4]
    slots = n_sp * cap
    peer = (i, y * 2 + 1 - c)
    straight = (1,)
    bounds = ((0, n_sp // 2), (n_sp // 2, 3 * n_sp // 4), (3 * n_sp // 4, n_sp))
    scope = jax.named_scope

    def columns(g):
        return pl.ds(pl.multiple_of(g * dg, dg), dg)

    def mate(k):
        to, bit = i, 1
        while bit <= k:
            if k & bit:
                to = to + bit * (1 - 2 * ((i // bit) % 2))
            bit *= 2
        return to

    def y_up(q):
        return lax.rem(y + q, ny)

    def remote(src, dst, s, r, who):
        return pltpu.make_async_remote_copy(
            src_ref=src, dst_ref=dst, send_sem=s, recv_sem=r, device_id=who, device_id_type=MESH
        )

    barrier = pltpu.get_barrier_semaphore()
    for k in range(1, n_sp):
        pl.semaphore_signal(barrier, inc=1, device_id=(mate(k), t), device_id_type=MESH)
    for k in range(1, n_tp):
        pl.semaphore_signal(
            barrier, inc=1, device_id=(i, lax.rem(t + k, n_tp)), device_id_type=MESH
        )

    held = ((ids_h, ids), (wts_h, wts), (mix_h, mix), (og_h, og), (gb_h, gb), (st_h, st), (dc_h, dc))
    held = held + ((wg_h, wg), (wu_h, wu), (wd_h, wd), (wp_h, wp))
    loads = [pltpu.make_async_copy(a, b, w_sem.at[n]) for n, (a, b) in enumerate(held)]
    for load in loads:
        load.start()
    for load in loads[:4]:
        load.wait()

    with scope("build"):
        experts_iota = lax.broadcasted_iota(jnp.int32, (n_sp, tok), 0)
        named = jnp.zeros((n_sp, tok), F32)
        weight = jnp.zeros((n_sp, tok), F32)
        for k in range(ids.shape[0]):
            hit = ids[k : k + 1, :] == experts_iota
            named = jnp.where(hit, 1.0, named)
            weight = jnp.where(hit, wts[k : k + 1, :], weight)
        earlier = (
            lax.broadcasted_iota(jnp.int32, (tok, tok), 0)
            < lax.broadcasted_iota(jnp.int32, (tok, tok), 1)
        )
        place = dot(named.astype(BF16), jnp.where(earlier, 1.0, 0.0).astype(BF16), 1, 0)
        place = jnp.where(named > 0.5, place, -1.0).astype(jnp.int32)
        slot_iota = lax.broadcasted_iota(jnp.int32, (cap, tok), 0)
        for e in range(n_sp):
            here = jnp.where(place[e : e + 1, :] == slot_iota, 1.0, 0.0)
            slot_weight = jnp.sum(here * weight[e : e + 1, :], axis=1, keepdims=True)
            sel[e * cap : (e + 1) * cap, :] = here.astype(BF16)
            sw[e * cap : (e + 1) * cap, :] = jnp.broadcast_to(slot_weight, (cap, sw.shape[1]))
        chosen = sel[...]
        for q in range(ny):
            cols = columns(2 * y_up(q) + c)
            send[0, q] = dot(chosen, mix[:, cols], 1, 0).astype(BF16).reshape(n_sp, cap, dg)
            send[1, q] = (
                (dot(chosen, og[:, cols], 1, 0) * sw[:, 0:1]).astype(BF16).reshape(n_sp, cap, dg)
            )
    with scope("barrier"):
        pl.semaphore_wait(barrier, n_sp + n_tp - 2)

    pending = []

    def go(copy):
        copy.start()
        pending.append(copy)

    def groups(k):
        return range(ny) if k in straight else range(1)

    def dispatch(q, k):
        return remote(
            send.at[:, q, mate(k)],
            xc.at[:, 2 * y_up(q) + c, i],
            sp_s.at[q, k],
            sp_r.at[q, k],
            (mate(k), t),
        )

    for k in range(1, n_sp):
        for q in groups(k):
            go(dispatch(q, k))

    with scope("own"):
        mine = pl.ds(pl.multiple_of(i * cap, cap), cap)
        here, slot_weight = sel[mine, :], sw[mine, 0:1]
        for g in range(n_tp):
            cols = slice(g * dg, (g + 1) * dg)
            xc[0, g, i] = dot(here, mix[:, cols], 1, 0).astype(BF16)
            xc[1, g, i] = (dot(here, og[:, cols], 1, 0) * slot_weight).astype(BF16)
        for load in loads[4:7]:
            load.wait()
        ga[i] = (gb[...].astype(F32) * st[...]).astype(BF16)
    go(
        remote(
            st.at[pl.ds(tok - 8, 8)],
            pv,
            pv_sem.at[0],
            pv_sem.at[1],
            (lax.rem(i + 1, n_sp), t),
        )
    )
    pv_copy = pending[-1]

    def to_core(q, k):
        block = xc.at[:, 2 * y_up(q) + c, mate(k)]
        return remote(block, block, core_s.at[q, k], core_r.at[q, k], peer)

    def to_y(q, k):
        block = xc.at[:, t, mate(k)]
        return remote(block, block, y_s.at[q, k], y_r.at[q, k], (i, 2 * y_up(q) + c))

    def from_y(q, k):
        block = xc.at[:, 2 * y_up(ny - q) + c, mate(k)]
        return remote(block, block, y_s.at[q, k], y_r.at[q, k], (i, 2 * y_up(q) + c))

    def from_sp(q, k):
        return remote(
            send.at[:, q, mate(k)],
            xc.at[:, 2 * y_up(q) + c, mate(k)],
            sp_s.at[q, k],
            sp_r.at[q, k],
            (mate(k), t),
        )

    def from_core(q, k):
        block = xc.at[:, 2 * y_up(q) + 1 - c, mate(k)]
        return remote(block, block, core_s.at[q, k], core_r.at[q, k], peer)

    def chunk(m):
        return [k for k in range(*bounds[m]) if k]

    def rows_of_chunk(m):
        first, end = bounds[m]
        return pl.ds(first * cap, (end - first) * cap)

    def spread(ks):
        for k in ks:
            with scope(f"spread{k}"):
                for q in groups(k):
                    from_sp(q, k).wait_recv()
                if k not in straight:
                    for q in range(1, ny):
                        go(to_y(q, k))
                for q in groups(k):
                    go(to_core(q, k))

    def hand_on(ks):
        for k in ks:
            if k in straight:
                continue
            with scope(f"hand{k}"):
                for q in range(1, ny):
                    from_y(q, k).wait_recv()
                    go(to_core(ny - q, k))

    def arrived(m):
        with scope(f"arr{m}"):
            for k in chunk(m):
                for q in range(ny):
                    from_core(q, k).wait_recv()

    def expert(m):
        order = [mate(k) for k in range(*bounds[m])]

        def rows_of(which, g):
            return jnp.concatenate([xc[which, g, s] for s in order], axis=0)

        gate = up = hg = None
        for g in range(n_tp):
            cols = slice(g * dg, (g + 1) * dg)
            x, cot = rows_of(0, g), rows_of(1, g)
            parts = (dot(x, wg[:, cols], 1, 1), dot(x, wu[:, cols], 1, 1), dot(cot, wd[:, cols], 1, 1))
            if g == 0:
                gate, up, hg = parts
            else:
                gate, up, hg = gate + parts[0], up + parts[1], hg + parts[2]
        s = jax.nn.sigmoid(gate)
        silu = gate * s
        hidden = (silu * up).astype(BF16)
        up_grad = (hg * silu).astype(BF16)
        gate_grad = (hg * up * s * (1.0 + gate * (1.0 - s))).astype(BF16)
        for q, src in enumerate(order):
            part = slice(q * cap, (q + 1) * cap)
            hid[src] = hidden[part]
            ug[src] = up_grad[part]
            gg[src] = gate_grad[part]
        return gate_grad, up_grad

    def partial(gate_grad, up_grad, g):
        cols = columns(g)
        return (dot(gate_grad, wg[:, cols], 1, 0) + dot(up_grad, wu[:, cols], 1, 0)).astype(BF16)

    def swap_core(m, q):
        rows = rows_of_chunk(m)
        return remote(pb.at[q, rows], rc.at[q, rows], pc_s.at[m, q], pc_r.at[m, q], peer)

    def swap_y(m, q):
        rows = rows_of_chunk(m)
        return remote(
            qb.at[q, rows], ry.at[q, rows], py_s.at[m, q], py_r.at[m, q], (i, 2 * y_up(q) + c)
        )

    def run(m):
        arrived(m)
        with scope(f"exp{m}"):
            grads = expert(m)
        rows = rows_of_chunk(m)
        with scope(f"part{m}"):
            for q in list(range(1, ny)) + [0]:
                pb[q, rows] = partial(*grads, 2 * y_up(q) + 1 - c)
                go(swap_core(m, q))
            for q in list(range(1, ny)) + [0]:
                po[q, rows] = partial(*grads, 2 * y_up(q) + c)

    def fold_core(m):
        rows = rows_of_chunk(m)
        with scope(f"foldc{m}"):
            for q in range(1, ny):
                swap_core(m, q).wait_recv()
                qb[q, rows] = (po[q, rows].astype(F32) + rc[q, rows].astype(F32)).astype(BF16)
                go(swap_y(m, q))

    def home(k):
        return remote(
            fb.at[pl.ds(k * cap, cap)], ret.at[i], ret_s.at[k], ret_r.at[k], (mate(k), t)
        )

    def fold_y(m):
        rows = rows_of_chunk(m)
        with scope(f"foldy{m}"):
            swap_core(m, 0).wait_recv()
            total = po[0, rows].astype(F32) + rc[0, rows].astype(F32)
            for q in range(1, ny):
                swap_y(m, q).wait_recv()
                total = total + ry[q, rows].astype(F32)
            total = total.astype(BF16)
            fb[rows] = total
            if m == 0:
                ret[i] = total[:cap]
            for k in chunk(m):
                go(home(k))

    def weight_grad(left, which, out):
        with scope("wgrad"):
            a = left[...].reshape(slots, left.shape[2])
            for g in range(n_tp):
                b = xc[which, g].reshape(slots, dg)
                out[:, g * dg : (g + 1) * dg] = dot(a, b, 0, 0).astype(BF16)

    def share_gated(k):
        return remote(ga.at[i], ga.at[i], ga_s.at[k], ga_r.at[k], (mate(k), t))

    def get_gated(k):
        return remote(ga.at[i], ga.at[mate(k)], ga_s.at[k], ga_r.at[k], (mate(k), t))

    def pass_gated(k):
        block = ga.at[mate(k)]
        return remote(block, block, ga_s.at[k + 1], ga_r.at[k + 1], (mate(1), t))

    def passed_gated(k):
        block = ga.at[mate(k + 1)]
        return remote(block, block, ga_s.at[k + 1], ga_r.at[k + 1], (mate(1), t))

    far = [k for k in range(2, n_sp, 2)]

    near = chunk(0)
    spread(near[1:])
    spread(near[:1])
    spread(chunk(1))
    hand_on(chunk(0))
    for load in loads[7:]:
        load.wait()
    run(0)
    spread(chunk(2))
    fold_core(0)
    for k in far:
        go(share_gated(k))
    hand_on(chunk(1))
    run(1)
    fold_core(1)
    hand_on(chunk(2))
    fold_y(0)
    run(2)
    fold_core(2)
    fold_y(1)
    weight_grad(gg, 0, dwg)
    fold_y(2)
    weight_grad(ug, 0, dwu)
    weight_grad(hid, 1, dwd)
    with scope("gated"):
        for k in range(0, n_sp, 2):
            if k:
                get_gated(k).wait_recv()
            go(pass_gated(k))

    def from_expert(k):
        return remote(
            fb.at[pl.ds(k * cap, cap)],
            ret.at[mate(k)],
            ret_s.at[k],
            ret_r.at[k],
            (mate(k), t),
        )

    for k in range(1, n_sp):
        with scope(f"ret{k}"):
            from_expert(k).wait_recv()
    with scope("mid"):
        routed = dot(ret[...].reshape(slots, dg), sel[...], 0, 0)
        mid = (og[:, columns(t)].astype(F32).T + routed).astype(BF16)
        mt[t] = mid

    def mid_core(q):
        block = mt.at[2 * y_up(q) + c]
        return remote(block, block, mtc_s.at[q], mtc_r.at[q], peer)

    def mid_from_core(q):
        block = mt.at[2 * y_up(q) + 1 - c]
        return remote(block, block, mtc_s.at[q], mtc_r.at[q], peer)

    def mid_y(q):
        return remote(mt.at[t], mt.at[t], mty_s.at[q], mty_r.at[q], (i, 2 * y_up(q) + c))

    def mid_from_y(q):
        block = mt.at[2 * y_up(ny - q) + c]
        return remote(block, block, mty_s.at[q], mty_r.at[q], (i, 2 * y_up(q) + c))

    for q in range(1, ny):
        go(mid_y(q))
    go(mid_core(0))

    row = lax.broadcasted_iota(jnp.int32, dc.shape, 0)
    decay = dc[...]
    head = decay[0:1, :]
    factor = jnp.where(row < tok - 1, pltpu.roll(decay, tok - 1, 0), 1.0)
    with scope("midx"):
        for q in range(1, ny):
            mid_from_y(q).wait_recv()
            go(mid_core(ny - q))
        for q in range(ny):
            mid_from_core(q).wait_recv()

    share = 2 * mr.shape[2]
    per = dg // share if dg >= share else 1

    part = share // 2

    def rows_for(s, h):
        first = (s % per) * share + h * part
        return mt.at[s // per, pl.ds(pl.multiple_of(first, part), part)]

    def share_rows(k):
        return remote(rows_for(mate(k), c), mr.at[i, c], mr_s.at[k], mr_r.at[k], (mate(k), t))

    def get_rows(k):
        return remote(
            rows_for(mate(k), c), mr.at[mate(k), c], mr_s.at[k], mr_r.at[k], (mate(k), t)
        )

    def swap_rows(k, h):
        block = mr.at[mate(k), h]
        return remote(block, block, mrc_s.at[k], mrc_r.at[k], peer)

    for k in range(n_sp - 1, 0, -1):
        go(share_rows(k))

    with scope("scan"):
        act = dot(mt[...].reshape(n_tp * dg, tok), wp[...], 0, 0)
        grad = act * gb[...].astype(F32)
        gbr[...] = (act * st[...]).astype(BF16)
        step = 1
        while step < tok:
            inside = row < tok - step
            grad = grad + jnp.where(inside, factor * pltpu.roll(grad, tok - step, 0), 0.0)
            factor = factor * jnp.where(inside, pltpu.roll(factor, tok - step, 0), 1.0)
            step *= 2
        pair = jnp.concatenate([head * factor[0:1, :], head * grad[0:1, :]], axis=0)
        pair = jnp.concatenate([pair, jnp.zeros((6, pair.shape[1]), F32)], axis=0)
        cs[...] = pair
        cr[i] = pair

    def share_carry(k):
        return remote(cs, cr.at[i], c_s.at[k], c_r.at[k], (mate(k), t))

    def get_carry(k):
        return remote(cs, cr.at[mate(k)], c_s.at[k], c_r.at[k], (mate(k), t))

    for k in range(1, n_sp):
        go(share_carry(k))
    for h in range(2):
        mr[i, h] = rows_for(i, h)[...]

    for k in range(1, n_sp):
        with scope(f"rows{k}"):
            get_rows(k).wait_recv()
            go(swap_rows(k, c))
    with scope("passed"):
        for k in range(0, n_sp, 2):
            passed_gated(k).wait_recv()
    with scope("gproj"):
        total = None
        for k in range(n_sp):
            if k:
                swap_rows(k, 1 - c).wait_recv()
            src = mate(k)
            term = dot(mr[src].reshape(share, tok), ga[src], 1, 0)
            total = term if total is None else total + term
        gproj[...] = total

    with scope("carry"):
        for k in range(1, n_sp):
            get_carry(k).wait_recv()
        carry = jnp.zeros((1, pair.shape[1]), F32)
        for s in range(n_sp - 1, 0, -1):
            carry = jnp.where(s > i, cr[s, 1:2, :] + cr[s, 0:1, :] * carry, carry)
        drive = grad + factor * carry
        gdr[...] = drive
        pv_copy.wait_recv()
        states = st[...]
        last = jnp.where(i > 0, pv[7:8, :], 0.0)
        previous = jnp.where(row == 0, last, pltpu.roll(states, 1, 0))
        gdc[...] = drive * previous

    with scope("drain"):
        for copy in pending:
            copy.wait_send()


def settle(count, *refs):
    ins, outs, sem = refs[:count], refs[count : 2 * count], refs[2 * count]
    puts = [pltpu.make_async_copy(ins[n], outs[n], sem.at[n]) for n in range(count)]
    for put in puts:
        put.start()
    for put in puts:
        put.wait()


def local(
    mixer_out,
    out_grad,
    route_ids,
    route_weights,
    gate_branch,
    states,
    decay,
    w_proj,
    w_gate,
    w_up,
    w_down,
):
    tok, width = mixer_out.shape
    top = route_ids.shape[1]
    n_sp, n_tp = lax.axis_size("sp"), lax.axis_size("tp")
    ny = n_tp // 2
    assert w_gate.shape[0] == 1
    cap = 2 * top * tok // n_sp
    dg = width // n_tp
    hidden = w_gate.shape[1]
    channels = states.shape[1]
    share = width // n_sp
    vmem = pl.BlockSpec(memory_space=pltpu.VMEM)
    hbm = pl.BlockSpec(memory_space=pltpu.HBM)
    dma = pltpu.SemaphoreType.DMA
    weight = (hidden, width)
    outs = pl.pallas_call(
        functools.partial(kernel, n_sp, n_tp),
        out_shape=[jax.ShapeDtypeStruct(weight, BF16)] * 3
        + [
            jax.ShapeDtypeStruct((share, channels), F32),
            jax.ShapeDtypeStruct((tok, channels), BF16),
            jax.ShapeDtypeStruct((tok, channels), F32),
            jax.ShapeDtypeStruct((tok, channels), F32),
        ],
        in_specs=[hbm] * 11,
        out_specs=[vmem] * 7,
        scratch_shapes=[
            pltpu.VMEM((top, tok), jnp.int32),
            pltpu.VMEM((top, tok), F32),
            pltpu.VMEM((tok, width), BF16),
            pltpu.VMEM((tok, width), BF16),
            pltpu.VMEM((tok, channels), BF16),
            pltpu.VMEM((tok, channels), F32),
            pltpu.VMEM((tok, channels), F32),
            pltpu.VMEM((width, channels), BF16),
            *([pltpu.VMEM(weight, BF16)] * 3),
            pltpu.VMEM((n_sp * cap, tok), BF16),
            pltpu.VMEM((n_sp * cap, 128), F32),
            pltpu.VMEM((2, ny, n_sp, cap, dg), BF16),
            pltpu.VMEM((2, n_tp, n_sp, cap, dg), BF16),
            pltpu.VMEM((n_sp, tok, channels), BF16),
            pltpu.VMEM((8, channels), F32),
            *([pltpu.VMEM((n_sp, cap, hidden), BF16)] * 3),
            *([pltpu.VMEM((ny, n_sp * cap, dg), BF16)] * 5),
            pltpu.VMEM((n_sp * cap, dg), BF16),
            pltpu.VMEM((n_sp, cap, dg), BF16),
            pltpu.VMEM((n_tp, dg, tok), BF16),
            pltpu.VMEM((n_sp, 2, share // 2, tok), BF16),
            pltpu.VMEM((8, channels), F32),
            pltpu.VMEM((n_sp, 8, channels), F32),
            dma((11,)),
            *([dma((ny, n_sp))] * 6),
            dma((n_sp,)),
            dma((n_sp,)),
            dma((2,)),
            *([dma((3, ny))] * 4),
            dma((n_sp,)),
            dma((n_sp,)),
            *([dma((ny,))] * 4),
            *([dma((n_sp,))] * 6),
        ],
        compiler_params=pltpu.CompilerParams(
            collective_id=0, has_side_effects=True, vmem_limit_bytes=LIMIT
        ),
    )(
        *(
            pltpu.with_memory_space_constraint(x, pltpu.HBM)
            for x in (
                route_ids.T,
                route_weights.T,
                mixer_out,
                out_grad,
                gate_branch,
                states,
                decay,
                w_proj,
                w_gate[0],
                w_up[0],
                w_down[0],
            )
        )
    )
    count = len(outs)
    outs = pl.pallas_call(
        functools.partial(settle, count),
        out_shape=[jax.ShapeDtypeStruct(o.shape, o.dtype) for o in outs],
        in_specs=[vmem] * count,
        out_specs=[hbm] * count,
        scratch_shapes=[dma((count,))],
        compiler_params=pltpu.CompilerParams(vmem_limit_bytes=LIMIT),
    )(*outs)
    return (outs[0][None], outs[1][None], outs[2][None], *outs[3:])


def solution(mesh):
    placed = (
        P("sp", None),
        P("sp", None),
        P("sp", None),
        P("sp", None),
        P("sp", "tp"),
        P("sp", "tp"),
        P("sp", "tp"),
        P(None, "tp"),
        P("sp", "tp", None),
        P("sp", "tp", None),
        P("sp", "tp", None),
    )
    return jax.shard_map(
        local,
        mesh=mesh,
        in_specs=placed,
        out_specs=(
            P("sp", "tp", None),
            P("sp", "tp", None),
            P("sp", "tp", None),
            P("sp", "tp"),
            P("sp", "tp"),
            P("sp", "tp"),
            P("sp", "tp"),
        ),
        check_vma=False,
    )
```

time: 91.7 us -> 80.3 us (0.88)
  Pallas kernels: 90.6 us -> 79.5 us
    pallas_call x1, Pallas kernels: 84.6 us -> 76.5 us  [local(): pl.pallas_call(functools.partial(kernel, n_sp, n_tp), out_shape=[jax.Shap...]
    pallas_call x1, Pallas kernels: 6.03 us -> 3.05 us  [local(): pl.pallas_call(functools.partial(settle, count), out_shape=[jax.ShapeDtyp...]
where the time goes in v1:
time: 80.3 us; the launch traced here: 80.2 us
  Pallas kernels  79.5 us (99%)
    pallas_call x1, Pallas kernels, local(): pl.pallas_call(functools.partial(kernel, n_sp, n_tp), out_shape=[jax.Shap...  76.5 us
    pallas_call x1, Pallas kernels, local(): pl.pallas_call(functools.partial(settle, count), out_shape=[jax.ShapeDtyp...  3.05 us

profile of v1, /device:TPU:0, one launch (start us, length us, event | category | flops | bytes accessed | tf_op | source)
XLA Modules:
  0.0 80.2 jit_solution(1717059820500844669)
XLA Ops:
  0.6 76.5 %shard_map.162 = (bf16[512,2048]{1,0:T(8,128)(2,1)S(1)}, bf16[512,2048]{1,0:T(8,128)(2,1)S(1)}, bf16[512,2048]{1,0:T(8,128)(2,1)S(1)}, f32[256,512]{1,0:T(8,128)...) custom-call(s32[2,128]{1,0:T(2,128)} %bitcast.11, f32[2,128]{1,0:T(2,128)} %bitcast.12, ...), custom_call_target="tpu_custom_call" | custom-call | tf_op jit(solution)/shard_map/pallas_call | solution.py:581
  77.1 3.1 %shard_map.163 = (bf16[512,2048]{1,0:T(8,128)(2,1)}, bf16[512,2048]{1,0:T(8,128)(2,1)}, bf16[512,2048]{1,0:T(8,128)(2,1)}, f32[256,512]{1,0:T(8,128)}, bf16[128,...) custom-call(bf16[512,2048]{1,0:T(8,128)(2,1)S(1)} %get-tuple-element.21.refs_0_, ...), custom_call_target="tpu_custom_call" | custom-call | tf_op jit(solution)/shard_map/pallas_call | solution.py:649

commit v2 on v1

--- a/solution.py
+++ b/solution.py
@@ -70,31 +70,15 @@
     cs,
     cr,
     w_sem,
-    sp_s,
+    put,
+    one_r,
     sp_r,
-    core_s,
     core_r,
-    y_s,
     y_r,
-    ga_s,
-    ga_r,
-    pv_sem,
-    pc_s,
     pc_r,
-    py_s,
     py_r,
-    ret_s,
-    ret_r,
-    mtc_s,
-    mtc_r,
-    mty_s,
     mty_r,
-    mr_s,
     mr_r,
-    mrc_s,
-    mrc_r,
-    c_s,
-    c_r,
 ):
     i = lax.axis_index("sp")
     t = lax.axis_index("tp")
@@ -106,7 +90,9 @@
     slots = n_sp * cap
     peer = (i, y * 2 + 1 - c)
     straight = (1,)
+    quarter = n_sp // 4
     bounds = ((0, n_sp // 2), (n_sp // 2, 3 * n_sp // 4), (3 * n_sp // 4, n_sp))
+    pieces = ((0, 1), (2,), (3,))
     scope = jax.named_scope
 
     def columns(g):
@@ -127,6 +113,9 @@
         return pltpu.make_async_remote_copy(
             src_ref=src, dst_ref=dst, send_sem=s, recv_sem=r, device_id=who, device_id_type=MESH
         )
+
+    def took(ref, sem):
+        remote(ref, ref, sem, sem, peer).wait_recv()
 
     barrier = pltpu.get_barrier_semaphore()
     for k in range(1, n_sp):
@@ -174,12 +163,6 @@
     with scope("barrier"):
         pl.semaphore_wait(barrier, n_sp + n_tp - 2)
 
-    pending = []
-
-    def go(copy):
-        copy.start()
-        pending.append(copy)
-
     def groups(k):
         return range(ny) if k in straight else range(1)
 
@@ -187,14 +170,14 @@
         return remote(
             send.at[:, q, mate(k)],
             xc.at[:, 2 * y_up(q) + c, i],
-            sp_s.at[q, k],
-            sp_r.at[q, k],
+            put.at[0 if q == 0 else 1],
+            sp_r.at[k if q == 0 else n_sp + q - 1],
             (mate(k), t),
         )
 
     for k in range(1, n_sp):
         for q in groups(k):
-            go(dispatch(q, k))
+            dispatch(q, k).start()
 
     with scope("own"):
         mine = pl.ds(pl.multiple_of(i * cap, cap), cap)
@@ -206,59 +189,48 @@
         for load in loads[4:7]:
             load.wait()
         ga[i] = (gb[...].astype(F32) * st[...]).astype(BF16)
-    go(
-        remote(
-            st.at[pl.ds(tok - 8, 8)],
-            pv,
-            pv_sem.at[0],
-            pv_sem.at[1],
-            (lax.rem(i + 1, n_sp), t),
-        )
+    pv_copy = remote(
+        st.at[pl.ds(tok - 8, 8)], pv, put.at[2], one_r.at[0], (lax.rem(i + 1, n_sp), t)
     )
-    pv_copy = pending[-1]
+    pv_copy.start()
+
+    def chunk_of(k):
+        return [first <= k < end for first, end in bounds].index(True)
 
     def to_core(q, k):
         block = xc.at[:, 2 * y_up(q) + c, mate(k)]
-        return remote(block, block, core_s.at[q, k], core_r.at[q, k], peer)
+        return remote(block, block, put.at[3], core_r.at[chunk_of(k)], peer)
 
     def to_y(q, k):
         block = xc.at[:, t, mate(k)]
-        return remote(block, block, y_s.at[q, k], y_r.at[q, k], (i, 2 * y_up(q) + c))
+        return remote(block, block, put.at[4], y_r.at[q - 1, k], (i, 2 * y_up(q) + c))
 
     def from_y(q, k):
         block = xc.at[:, 2 * y_up(ny - q) + c, mate(k)]
-        return remote(block, block, y_s.at[q, k], y_r.at[q, k], (i, 2 * y_up(q) + c))
+        took(block, y_r.at[q - 1, k])
 
     def from_sp(q, k):
-        return remote(
-            send.at[:, q, mate(k)],
-            xc.at[:, 2 * y_up(q) + c, mate(k)],
-            sp_s.at[q, k],
-            sp_r.at[q, k],
-            (mate(k), t),
-        )
-
-    def from_core(q, k):
-        block = xc.at[:, 2 * y_up(q) + 1 - c, mate(k)]
-        return remote(block, block, core_s.at[q, k], core_r.at[q, k], peer)
+        took(xc.at[:, 2 * y_up(q) + c, mate(k)], sp_r.at[k if q == 0 else n_sp + q - 1])
 
     def chunk(m):
         return [k for k in range(*bounds[m]) if k]
 
-    def rows_of_chunk(m):
-        first, end = bounds[m]
-        return pl.ds(first * cap, (end - first) * cap)
+    def piece(p):
+        return range(p * quarter, (p + 1) * quarter)
+
+    def rows_of(p):
+        return pl.ds(p * quarter * cap, quarter * cap)
 
     def spread(ks):
         for k in ks:
             with scope(f"spread{k}"):
                 for q in groups(k):
-                    from_sp(q, k).wait_recv()
+                    from_sp(q, k)
                 if k not in straight:
                     for q in range(1, ny):
-                        go(to_y(q, k))
+                        to_y(q, k).start()
                 for q in groups(k):
-                    go(to_core(q, k))
+                    to_core(q, k).start()
 
     def hand_on(ks):
         for k in ks:
@@ -266,25 +238,23 @@
                 continue
             with scope(f"hand{k}"):
                 for q in range(1, ny):
-                    from_y(q, k).wait_recv()
-                    go(to_core(ny - q, k))
+                    from_y(q, k)
+                    to_core(ny - q, k).start()
 
     def arrived(m):
         with scope(f"arr{m}"):
-            for k in chunk(m):
-                for q in range(ny):
-                    from_core(q, k).wait_recv()
+            took(xc.at[:, :ny, : len(chunk(m))], core_r.at[m])
 
     def expert(m):
         order = [mate(k) for k in range(*bounds[m])]
 
-        def rows_of(which, g):
+        def gathered(which, g):
             return jnp.concatenate([xc[which, g, s] for s in order], axis=0)
 
         gate = up = hg = None
         for g in range(n_tp):
             cols = slice(g * dg, (g + 1) * dg)
-            x, cot = rows_of(0, g), rows_of(1, g)
+            x, cot = gathered(0, g), gathered(1, g)
             parts = (dot(x, wg[:, cols], 1, 1), dot(x, wu[:, cols], 1, 1), dot(cot, wd[:, cols], 1, 1))
             if g == 0:
                 gate, up, hg = parts
@@ -306,55 +276,57 @@
         cols = columns(g)
         return (dot(gate_grad, wg[:, cols], 1, 0) + dot(up_grad, wu[:, cols], 1, 0)).astype(BF16)
 
-    def swap_core(m, q):
-        rows = rows_of_chunk(m)
-        return remote(pb.at[q, rows], rc.at[q, rows], pc_s.at[m, q], pc_r.at[m, q], peer)
-
-    def swap_y(m, q):
-        rows = rows_of_chunk(m)
+    def swap_core(p, q):
+        rows = rows_of(p)
+        return remote(pb.at[q, rows], rc.at[q, rows], put.at[5], pc_r.at[p, q], peer)
+
+    def swap_y(p, q):
+        rows = rows_of(p)
         return remote(
-            qb.at[q, rows], ry.at[q, rows], py_s.at[m, q], py_r.at[m, q], (i, 2 * y_up(q) + c)
+            qb.at[q, rows], ry.at[q, rows], put.at[6], py_r.at[p, q - 1], (i, 2 * y_up(q) + c)
         )
 
     def run(m):
         arrived(m)
         with scope(f"exp{m}"):
             grads = expert(m)
-        rows = rows_of_chunk(m)
+        rows = pl.ds(bounds[m][0] * cap, (bounds[m][1] - bounds[m][0]) * cap)
         with scope(f"part{m}"):
             for q in list(range(1, ny)) + [0]:
                 pb[q, rows] = partial(*grads, 2 * y_up(q) + 1 - c)
-                go(swap_core(m, q))
+                for p in reversed(pieces[m]):
+                    swap_core(p, q).start()
             for q in list(range(1, ny)) + [0]:
                 po[q, rows] = partial(*grads, 2 * y_up(q) + c)
 
-    def fold_core(m):
-        rows = rows_of_chunk(m)
-        with scope(f"foldc{m}"):
+    def fold_core(p):
+        rows = rows_of(p)
+        with scope(f"foldc{p}"):
             for q in range(1, ny):
-                swap_core(m, q).wait_recv()
+                took(rc.at[q, rows], pc_r.at[p, q])
                 qb[q, rows] = (po[q, rows].astype(F32) + rc[q, rows].astype(F32)).astype(BF16)
-                go(swap_y(m, q))
+                swap_y(p, q).start()
 
     def home(k):
         return remote(
-            fb.at[pl.ds(k * cap, cap)], ret.at[i], ret_s.at[k], ret_r.at[k], (mate(k), t)
-        )
-
-    def fold_y(m):
-        rows = rows_of_chunk(m)
-        with scope(f"foldy{m}"):
-            swap_core(m, 0).wait_recv()
+            fb.at[pl.ds(k * cap, cap)], ret.at[i], put.at[7], one_r.at[1], (mate(k), t)
+        )
+
+    def fold_y(p):
+        rows = rows_of(p)
+        with scope(f"foldy{p}"):
+            took(rc.at[0, rows], pc_r.at[p, 0])
             total = po[0, rows].astype(F32) + rc[0, rows].astype(F32)
             for q in range(1, ny):
-                swap_y(m, q).wait_recv()
+                took(ry.at[q, rows], py_r.at[p, q - 1])
                 total = total + ry[q, rows].astype(F32)
             total = total.astype(BF16)
             fb[rows] = total
-            if m == 0:
+            if p == 0:
                 ret[i] = total[:cap]
-            for k in chunk(m):
-                go(home(k))
+            for k in piece(p):
+                if k:
+                    home(k).start()
 
     def weight_grad(left, which, out):
         with scope("wgrad"):
@@ -364,18 +336,11 @@
                 out[:, g * dg : (g + 1) * dg] = dot(a, b, 0, 0).astype(BF16)
 
     def share_gated(k):
-        return remote(ga.at[i], ga.at[i], ga_s.at[k], ga_r.at[k], (mate(k), t))
-
-    def get_gated(k):
-        return remote(ga.at[i], ga.at[mate(k)], ga_s.at[k], ga_r.at[k], (mate(k), t))
+        return remote(ga.at[i], ga.at[i], put.at[8], one_r.at[2], (mate(k), t))
 
     def pass_gated(k):
         block = ga.at[mate(k)]
-        return remote(block, block, ga_s.at[k + 1], ga_r.at[k + 1], (mate(1), t))
-
-    def passed_gated(k):
-        block = ga.at[mate(k + 1)]
-        return remote(block, block, ga_s.at[k + 1], ga_r.at[k + 1], (mate(1), t))
+        return remote(block, block, put.at[8], one_r.at[3], (mate(1), t))
 
     far = [k for k in range(2, n_sp, 2)]
 
@@ -388,39 +353,30 @@
         load.wait()
     run(0)
     spread(chunk(2))
-    fold_core(0)
+    fold_core(1)
     for k in far:
-        go(share_gated(k))
+        share_gated(k).start()
     hand_on(chunk(1))
     run(1)
-    fold_core(1)
+    fold_core(2)
+    fold_core(0)
     hand_on(chunk(2))
+    run(2)
+    fold_core(3)
+    fold_y(1)
+    fold_y(2)
     fold_y(0)
-    run(2)
-    fold_core(2)
-    fold_y(1)
     weight_grad(gg, 0, dwg)
-    fold_y(2)
+    fold_y(3)
     weight_grad(ug, 0, dwu)
     weight_grad(hid, 1, dwd)
     with scope("gated"):
+        took(ga.at[pl.ds(0, len(far))], one_r.at[2])
         for k in range(0, n_sp, 2):
-            if k:
-                get_gated(k).wait_recv()
-            go(pass_gated(k))
-
-    def from_expert(k):
-        return remote(
-            fb.at[pl.ds(k * cap, cap)],
-            ret.at[mate(k)],
-            ret_s.at[k],
-            ret_r.at[k],
-            (mate(k), t),
-        )
-
-    for k in range(1, n_sp):
-        with scope(f"ret{k}"):
-            from_expert(k).wait_recv()
+            pass_gated(k).start()
+
+    with scope("ret"):
+        took(ret.at[pl.ds(1, n_sp - 1)], one_r.at[1])
     with scope("mid"):
         routed = dot(ret[...].reshape(slots, dg), sel[...], 0, 0)
         mid = (og[:, columns(t)].astype(F32).T + routed).astype(BF16)
@@ -428,57 +384,49 @@
 
     def mid_core(q):
         block = mt.at[2 * y_up(q) + c]
-        return remote(block, block, mtc_s.at[q], mtc_r.at[q], peer)
-
-    def mid_from_core(q):
-        block = mt.at[2 * y_up(q) + 1 - c]
-        return remote(block, block, mtc_s.at[q], mtc_r.at[q], peer)
+        return remote(block, block, put.at[9], one_r.at[4], peer)
 
     def mid_y(q):
-        return remote(mt.at[t], mt.at[t], mty_s.at[q], mty_r.at[q], (i, 2 * y_up(q) + c))
-
-    def mid_from_y(q):
-        block = mt.at[2 * y_up(ny - q) + c]
-        return remote(block, block, mty_s.at[q], mty_r.at[q], (i, 2 * y_up(q) + c))
+        return remote(mt.at[t], mt.at[t], put.at[9], mty_r.at[q - 1], (i, 2 * y_up(q) + c))
 
     for q in range(1, ny):
-        go(mid_y(q))
-    go(mid_core(0))
-
+        mid_y(q).start()
+    mid_core(0).start()
+
+    part = mr.shape[2]
+    share = 2 * part
+    per = dg // share
+    others = [(1, n_sp // 2), (n_sp // 2, 3 * n_sp // 4), (3 * n_sp // 4, n_sp)]
+
+    def share_rows(k):
+        s = mate(k)
+        first = pl.multiple_of((s % per) * share + c * part, part)
+        group = [first <= k < end for first, end in others].index(True)
+        return remote(
+            mt.at[s // per, pl.ds(first, part)], mr.at[k, c], put.at[10], mr_r.at[group], (s, t)
+        )
+
+    def pass_rows(n):
+        with scope(f"rows{n}"):
+            first, end = others[n]
+            block = mr.at[pl.ds(first, end - first), c]
+            took(block, mr_r.at[n])
+            remote(block, block, put.at[11], one_r.at[6], peer).start()
+
+    width = dc.shape[1]
     row = lax.broadcasted_iota(jnp.int32, dc.shape, 0)
     decay = dc[...]
     head = decay[0:1, :]
     factor = jnp.where(row < tok - 1, pltpu.roll(decay, tok - 1, 0), 1.0)
     with scope("midx"):
         for q in range(1, ny):
-            mid_from_y(q).wait_recv()
-            go(mid_core(ny - q))
-        for q in range(ny):
-            mid_from_core(q).wait_recv()
-
-    share = 2 * mr.shape[2]
-    per = dg // share if dg >= share else 1
-
-    part = share // 2
-
-    def rows_for(s, h):
-        first = (s % per) * share + h * part
-        return mt.at[s // per, pl.ds(pl.multiple_of(first, part), part)]
-
-    def share_rows(k):
-        return remote(rows_for(mate(k), c), mr.at[i, c], mr_s.at[k], mr_r.at[k], (mate(k), t))
-
-    def get_rows(k):
-        return remote(
-            rows_for(mate(k), c), mr.at[mate(k), c], mr_s.at[k], mr_r.at[k], (mate(k), t)
-        )
-
-    def swap_rows(k, h):
-        block = mr.at[mate(k), h]
-        return remote(block, block, mrc_s.at[k], mrc_r.at[k], peer)
-
+            took(mt.at[2 * y_up(ny - q) + c], mty_r.at[q - 1])
+            mid_core(ny - q).start()
+
+    with scope("midc"):
+        took(mt.at[pl.ds(0, ny)], one_r.at[4])
     for k in range(n_sp - 1, 0, -1):
-        go(share_rows(k))
+        share_rows(k).start()
 
     with scope("scan"):
         act = dot(mt[...].reshape(n_tp * dg, tok), wp[...], 0, 0)
@@ -490,45 +438,43 @@
             grad = grad + jnp.where(inside, factor * pltpu.roll(grad, tok - step, 0), 0.0)
             factor = factor * jnp.where(inside, pltpu.roll(factor, tok - step, 0), 1.0)
             step *= 2
-        pair = jnp.concatenate([head * factor[0:1, :], head * grad[0:1, :]], axis=0)
-        pair = jnp.concatenate([pair, jnp.zeros((6, pair.shape[1]), F32)], axis=0)
-        cs[...] = pair
-        cr[i] = pair
+        cs[...] = jnp.zeros(cs.shape, F32)
+        for j in range(width // 128):
+            lanes = slice(j * 128, (j + 1) * 128)
+            cs[j : j + 1, :] = head[:, lanes] * factor[0:1, lanes]
+            cs[width // 128 + j : width // 128 + j + 1, :] = head[:, lanes] * grad[0:1, lanes]
 
     def share_carry(k):
-        return remote(cs, cr.at[i], c_s.at[k], c_r.at[k], (mate(k), t))
-
-    def get_carry(k):
-        return remote(cs, cr.at[mate(k)], c_s.at[k], c_r.at[k], (mate(k), t))
-
-    for k in range(1, n_sp):
-        go(share_carry(k))
-    for h in range(2):
-        mr[i, h] = rows_for(i, h)[...]
-
-    for k in range(1, n_sp):
-        with scope(f"rows{k}"):
-            get_rows(k).wait_recv()
-            go(swap_rows(k, c))
+        return remote(cs, cr.at[i], put.at[12], one_r.at[5], (mate(k), t))
+
+    for k in range(n_sp - 1, 0, -1):
+        share_carry(k).start()
+
+    for n in range(3):
+        pass_rows(n)
     with scope("passed"):
-        for k in range(0, n_sp, 2):
-            passed_gated(k).wait_recv()
+        took(ga.at[pl.ds(0, n_sp // 2)], one_r.at[3])
+    with scope("gproj0"):
+        own = mt[i // per, pl.ds(pl.multiple_of((i % per) * share, share), share)]
+        total = dot(own, ga[i], 1, 0)
+    with scope("rowsc"):
+        took(mr.at[pl.ds(1, n_sp - 1), 0], one_r.at[6])
     with scope("gproj"):
-        total = None
-        for k in range(n_sp):
-            if k:
-                swap_rows(k, 1 - c).wait_recv()
-            src = mate(k)
-            term = dot(mr[src].reshape(share, tok), ga[src], 1, 0)
-            total = term if total is None else total + term
+        for k in range(1, n_sp):
+            total = total + dot(mr[k].reshape(share, tok), ga[mate(k)], 1, 0)
         gproj[...] = total
 
     with scope("carry"):
-        for k in range(1, n_sp):
-            get_carry(k).wait_recv()
-        carry = jnp.zeros((1, pair.shape[1]), F32)
+        took(cr.at[pl.ds(1, n_sp - 1)], one_r.at[5])
+
+        def lane_row(s, first):
+            return jnp.concatenate(
+                [cr[s, first + j : first + j + 1, :] for j in range(width // 128)], axis=1
+            )
+
+        carry = jnp.zeros((1, width), F32)
         for s in range(n_sp - 1, 0, -1):
-            carry = jnp.where(s > i, cr[s, 1:2, :] + cr[s, 0:1, :] * carry, carry)
+            carry = jnp.where(s > i, lane_row(s, width // 128) + lane_row(s, 0) * carry, carry)
         drive = grad + factor * carry
         gdr[...] = drive
         pv_copy.wait_recv()
@@ -538,8 +484,19 @@
         gdc[...] = drive * previous
 
     with scope("drain"):
-        for copy in pending:
-            copy.wait_send()
+        took(xc.at[:, 0, pl.ds(1, n_sp - 1)], put.at[0])
+        took(xc.at[:, pl.ds(0, ny - 1), 0], put.at[1])
+        pv_copy.wait_send()
+        took(xc.at[:, pl.ds(0, ny), pl.ds(1, n_sp - 1)], put.at[3])
+        took(xc.at[:, pl.ds(0, ny - 1), pl.ds(2, n_sp - 2)], put.at[4])
+        took(pb, put.at[5])
+        took(qb.at[pl.ds(1, ny - 1)], put.at[6])
+        took(fb.at[pl.ds(cap, (n_sp - 1) * cap)], put.at[7])
+        took(ga.at[pl.ds(1, n_sp - 1)], put.at[8])
+        took(mt.at[pl.ds(1, n_tp - 1)], put.at[9])
+        took(mr.at[pl.ds(1, n_sp - 1), 0], put.at[10])
+        took(mr.at[pl.ds(1, n_sp - 1), 0], put.at[11])
+        took(cr.at[pl.ds(1, n_sp - 1)], put.at[12])
 
 
 def settle(count, *refs):
@@ -611,18 +568,18 @@
             pltpu.VMEM((n_sp, cap, dg), BF16),
             pltpu.VMEM((n_tp, dg, tok), BF16),
             pltpu.VMEM((n_sp, 2, share // 2, tok), BF16),
-            pltpu.VMEM((8, channels), F32),
-            pltpu.VMEM((n_sp, 8, channels), F32),
+            pltpu.VMEM((max(8, channels // 64), 128), F32),
+            pltpu.VMEM((n_sp, max(8, channels // 64), 128), F32),
             dma((11,)),
-            *([dma((ny, n_sp))] * 6),
-            dma((n_sp,)),
-            dma((n_sp,)),
-            dma((2,)),
-            *([dma((3, ny))] * 4),
-            dma((n_sp,)),
-            dma((n_sp,)),
-            *([dma((ny,))] * 4),
-            *([dma((n_sp,))] * 6),
+            dma((13,)),
+            dma((7,)),
+            dma((n_sp + ny - 1,)),
+            dma((3,)),
+            dma((ny - 1, n_sp)),
+            dma((4, ny)),
+            dma((4, ny - 1)),
+            dma((ny - 1,)),
+            dma((3,)),
         ],
         compiler_params=pltpu.CompilerParams(
             collective_id=0, has_side_effects=True, vmem_limit_bytes=LIMIT

time: 80.3 us -> 75.2 us (0.936)
  Pallas kernels: 79.5 us -> 74.4 us
    pallas_call x1, Pallas kernels: 76.5 us -> 71.3 us  [local(): pl.pallas_call(functools.partial(kernel, n_sp, n_tp), out_shape=[jax.Shap...]
where the time goes in v2:
time: 75.2 us; the launch traced here: 75 us
  Pallas kernels  74.4 us (99%)
    pallas_call x1, Pallas kernels, local(): pl.pallas_call(functools.partial(kernel, n_sp, n_tp), out_shape=[jax.Shap...  71.3 us
    pallas_call x1, Pallas kernels, local(): pl.pallas_call(functools.partial(settle, count), out_shape=[jax.ShapeDtyp...  3.05 us

profile of v2, /device:TPU:0, one launch (start us, length us, event | category | flops | bytes accessed | tf_op | source)
XLA Modules:
  0.0 75.0 jit_solution(15966717482462800156)
XLA Ops:
  0.6 71.3 %shard_map.162 = (bf16[512,2048]{1,0:T(8,128)(2,1)S(1)}, bf16[512,2048]{1,0:T(8,128)(2,1)S(1)}, bf16[512,2048]{1,0:T(8,128)(2,1)S(1)}, f32[256,512]{1,0:T(8,128)...) custom-call(s32[2,128]{1,0:T(2,128)} %bitcast.11, f32[2,128]{1,0:T(2,128)} %bitcast.12, ...), custom_call_target="tpu_custom_call" | custom-call | tf_op jit(solution)/shard_map/pallas_call | solution.py:538
  72.0 3.1 %shard_map.163 = (bf16[512,2048]{1,0:T(8,128)(2,1)}, bf16[512,2048]{1,0:T(8,128)(2,1)}, bf16[512,2048]{1,0:T(8,128)(2,1)}, f32[256,512]{1,0:T(8,128)}, bf16[128,...) custom-call(bf16[512,2048]{1,0:T(8,128)(2,1)S(1)} %get-tuple-element.21.refs_0_, ...), custom_call_target="tpu_custom_call" | custom-call | tf_op jit(solution)/shard_map/pallas_call | solution.py:606

commit v3 on v2

--- a/solution.py
+++ b/solution.py
@@ -10,6 +10,7 @@
 MESH = pl.DeviceIdType.MESH
 F32 = jnp.float32
 BF16 = jnp.bfloat16
+STRAIGHT = (1, 3)
 LIMIT = 44 * 1024 * 1024
 
 
@@ -79,6 +80,7 @@
     py_r,
     mty_r,
     mr_r,
+    ga_r,
 ):
     i = lax.axis_index("sp")
     t = lax.axis_index("tp")
@@ -89,7 +91,7 @@
     dg = xc.shape[4]
     slots = n_sp * cap
     peer = (i, y * 2 + 1 - c)
-    straight = (1,)
+    straight = STRAIGHT
     quarter = n_sp // 4
     bounds = ((0, n_sp // 2), (n_sp // 2, 3 * n_sp // 4), (3 * n_sp // 4, n_sp))
     pieces = ((0, 1), (2,), (3,))
@@ -154,12 +156,18 @@
             sel[e * cap : (e + 1) * cap, :] = here.astype(BF16)
             sw[e * cap : (e + 1) * cap, :] = jnp.broadcast_to(slot_weight, (cap, sw.shape[1]))
         chosen = sel[...]
-        for q in range(ny):
-            cols = columns(2 * y_up(q) + c)
-            send[0, q] = dot(chosen, mix[:, cols], 1, 0).astype(BF16).reshape(n_sp, cap, dg)
-            send[1, q] = (
-                (dot(chosen, og[:, cols], 1, 0) * sw[:, 0:1]).astype(BF16).reshape(n_sp, cap, dg)
-            )
+        cols = columns(t)
+        send[0, 0] = dot(chosen, mix[:, cols], 1, 0).astype(BF16).reshape(n_sp, cap, dg)
+        send[1, 0] = (
+            (dot(chosen, og[:, cols], 1, 0) * sw[:, 0:1]).astype(BF16).reshape(n_sp, cap, dg)
+        )
+        for k in straight:
+            to = mate(k)
+            at = pl.ds(pl.multiple_of(to * cap, cap), cap)
+            for q in range(1, ny):
+                cols = columns(2 * y_up(q) + c)
+                send[0, q, to] = dot(sel[at, :], mix[:, cols], 1, 0).astype(BF16)
+                send[1, q, to] = (dot(sel[at, :], og[:, cols], 1, 0) * sw[at, 0:1]).astype(BF16)
     with scope("barrier"):
         pl.semaphore_wait(barrier, n_sp + n_tp - 2)
 
@@ -171,7 +179,7 @@
             send.at[:, q, mate(k)],
             xc.at[:, 2 * y_up(q) + c, i],
             put.at[0 if q == 0 else 1],
-            sp_r.at[k if q == 0 else n_sp + q - 1],
+            sp_r.at[k if q == 0 else n_sp + straight.index(k) * (ny - 1) + q - 1],
             (mate(k), t),
         )
 
@@ -210,7 +218,7 @@
         took(block, y_r.at[q - 1, k])
 
     def from_sp(q, k):
-        took(xc.at[:, 2 * y_up(q) + c, mate(k)], sp_r.at[k if q == 0 else n_sp + q - 1])
+        took(xc.at[:, 2 * y_up(q) + c, mate(k)], sp_r.at[k if q == 0 else n_sp + straight.index(k) * (ny - 1) + q - 1])
 
     def chunk(m):
         return [k for k in range(*bounds[m]) if k]
@@ -335,14 +343,36 @@
                 b = xc[which, g].reshape(slots, dg)
                 out[:, g * dg : (g + 1) * dg] = dot(a, b, 0, 0).astype(BF16)
 
-    def share_gated(k):
-        return remote(ga.at[i], ga.at[i], put.at[8], one_r.at[2], (mate(k), t))
+    level = i // quarter
+
+    def gated_block(d):
+        return ga.at[i + d * quarter]
+
+    def send_gated(d, way):
+        block = gated_block(-d * way)
+        remote(block, block, put.at[8], ga_r.at[d, (1 - way) // 2], (i + way * quarter, t)).start()
+
+    def share_gated():
+        pl.when(level < 3)(lambda: send_gated(0, 1))
+        pl.when(level > 0)(lambda: send_gated(0, -1))
+
+    def relay_gated(d):
+        with scope(f"relay{d}"):
+
+            @pl.when(level >= d)
+            def _():
+                took(gated_block(-d), ga_r.at[d - 1, 0])
+                pl.when(level < 3)(lambda: send_gated(d, 1))
+
+            @pl.when(level + d < 4)
+            def _():
+                took(gated_block(d), ga_r.at[d - 1, 1])
+                pl.when(level > 0)(lambda: send_gated(d, -1))
 
     def pass_gated(k):
-        block = ga.at[mate(k)]
-        return remote(block, block, put.at[8], one_r.at[3], (mate(1), t))
-
-    far = [k for k in range(2, n_sp, 2)]
+        for n in range(4):
+            block = ga.at[n * quarter + i % quarter]
+            remote(block, block, put.at[12], one_r.at[3], (mate(k), t)).start()
 
     near = chunk(0)
     spread(near[1:])
@@ -354,15 +384,16 @@
     run(0)
     spread(chunk(2))
     fold_core(1)
-    for k in far:
-        share_gated(k).start()
+    share_gated()
     hand_on(chunk(1))
     run(1)
     fold_core(2)
     fold_core(0)
     hand_on(chunk(2))
+    relay_gated(1)
     run(2)
     fold_core(3)
+    relay_gated(2)
     fold_y(1)
     fold_y(2)
     fold_y(0)
@@ -371,9 +402,9 @@
     weight_grad(ug, 0, dwu)
     weight_grad(hid, 1, dwd)
     with scope("gated"):
-        took(ga.at[pl.ds(0, len(far))], one_r.at[2])
-        for k in range(0, n_sp, 2):
-            pass_gated(k).start()
+        relay_gated(3)
+        for k in range(1, quarter):
+            pass_gated(k)
 
     with scope("ret"):
         took(ret.at[pl.ds(1, n_sp - 1)], one_r.at[1])
@@ -445,7 +476,7 @@
             cs[width // 128 + j : width // 128 + j + 1, :] = head[:, lanes] * grad[0:1, lanes]
 
     def share_carry(k):
-        return remote(cs, cr.at[i], put.at[12], one_r.at[5], (mate(k), t))
+        return remote(cs, cr.at[i], put.at[13], one_r.at[5], (mate(k), t))
 
     for k in range(n_sp - 1, 0, -1):
         share_carry(k).start()
@@ -453,7 +484,7 @@
     for n in range(3):
         pass_rows(n)
     with scope("passed"):
-        took(ga.at[pl.ds(0, n_sp // 2)], one_r.at[3])
+        took(ga.at[pl.ds(0, 4 * (quarter - 1))], one_r.at[3])
     with scope("gproj0"):
         own = mt[i // per, pl.ds(pl.multiple_of((i % per) * share, share), share)]
         total = dot(own, ga[i], 1, 0)
@@ -485,18 +516,21 @@
 
     with scope("drain"):
         took(xc.at[:, 0, pl.ds(1, n_sp - 1)], put.at[0])
-        took(xc.at[:, pl.ds(0, ny - 1), 0], put.at[1])
+        took(xc.at[:, pl.ds(0, ny - 1), pl.ds(0, len(straight))], put.at[1])
         pv_copy.wait_send()
         took(xc.at[:, pl.ds(0, ny), pl.ds(1, n_sp - 1)], put.at[3])
-        took(xc.at[:, pl.ds(0, ny - 1), pl.ds(2, n_sp - 2)], put.at[4])
+        took(xc.at[:, pl.ds(0, ny - 1), pl.ds(0, n_sp - 1 - len(straight))], put.at[4])
         took(pb, put.at[5])
         took(qb.at[pl.ds(1, ny - 1)], put.at[6])
         took(fb.at[pl.ds(cap, (n_sp - 1) * cap)], put.at[7])
-        took(ga.at[pl.ds(1, n_sp - 1)], put.at[8])
+        middle = level * (3 - level) > 0
+        pl.when(middle)(lambda: took(ga.at[pl.ds(0, 5)], put.at[8]))
+        pl.when(jnp.logical_not(middle))(lambda: took(ga.at[0], put.at[8]))
+        took(ga.at[pl.ds(0, 4 * (quarter - 1))], put.at[12])
         took(mt.at[pl.ds(1, n_tp - 1)], put.at[9])
         took(mr.at[pl.ds(1, n_sp - 1), 0], put.at[10])
         took(mr.at[pl.ds(1, n_sp - 1), 0], put.at[11])
-        took(cr.at[pl.ds(1, n_sp - 1)], put.at[12])
+        took(cr.at[pl.ds(1, n_sp - 1)], put.at[13])
 
 
 def settle(count, *refs):
@@ -571,15 +605,16 @@
             pltpu.VMEM((max(8, channels // 64), 128), F32),
             pltpu.VMEM((n_sp, max(8, channels // 64), 128), F32),
             dma((11,)),
-            dma((13,)),
+            dma((14,)),
             dma((7,)),
-            dma((n_sp + ny - 1,)),
+            dma((n_sp + len(STRAIGHT) * (ny - 1),)),
             dma((3,)),
             dma((ny - 1, n_sp)),
             dma((4, ny)),
             dma((4, ny - 1)),
             dma((ny - 1,)),
             dma((3,)),
+            dma((4, 2)),
         ],
         compiler_params=pltpu.CompilerParams(
             collective_id=0, has_side_effects=True, vmem_limit_bytes=LIMIT

time: 75.2 us -> 74.2 us (0.987)
  Pallas kernels: 74.4 us -> 73.2 us
    pallas_call x1, Pallas kernels: 71.3 us -> 70.1 us  [local(): pl.pallas_call(functools.partial(kernel, n_sp, n_tp), out_shape=[jax.Shap...]
where the time goes in v3:
time: 74.2 us; the launch traced here: 73.8 us
  Pallas kernels  73.2 us (99%)
    pallas_call x1, Pallas kernels, local(): pl.pallas_call(functools.partial(kernel, n_sp, n_tp), out_shape=[jax.Shap...  70.1 us
    pallas_call x1, Pallas kernels, local(): pl.pallas_call(functools.partial(settle, count), out_shape=[jax.ShapeDtyp...  3.05 us

profile of v3, /device:TPU:0, one launch (start us, length us, event | category | flops | bytes accessed | tf_op | source)
XLA Modules:
  0.0 73.8 jit_solution(5566295316270739529)
XLA Ops:
  0.6 70.1 %shard_map.162 = (bf16[512,2048]{1,0:T(8,128)(2,1)S(1)}, bf16[512,2048]{1,0:T(8,128)(2,1)S(1)}, bf16[512,2048]{1,0:T(8,128)(2,1)S(1)}, f32[256,512]{1,0:T(8,128)...) custom-call(s32[2,128]{1,0:T(2,128)} %bitcast.11, f32[2,128]{1,0:T(2,128)} %bitcast.12, ...), custom_call_target="tpu_custom_call" | custom-call | tf_op jit(solution)/shard_map/pallas_call | solution.py:572
  70.7 3.1 %shard_map.163 = (bf16[512,2048]{1,0:T(8,128)(2,1)}, bf16[512,2048]{1,0:T(8,128)(2,1)}, bf16[512,2048]{1,0:T(8,128)(2,1)}, f32[256,512]{1,0:T(8,128)}, bf16[128,...) custom-call(bf16[512,2048]{1,0:T(8,128)(2,1)S(1)} %get-tuple-element.21.refs_0_, ...), custom_call_target="tpu_custom_call" | custom-call | tf_op jit(solution)/shard_map/pallas_call | solution.py:641

commit v4 on v3

--- a/solution.py
+++ b/solution.py
@@ -352,9 +352,15 @@
         block = gated_block(-d * way)
         remote(block, block, put.at[8], ga_r.at[d, (1 - way) // 2], (i + way * quarter, t)).start()
 
+    def pass_gated(d):
+        block = gated_block(d)
+        for k in range(1, quarter):
+            remote(block, block, put.at[12], one_r.at[3], (mate(k), t)).start()
+
     def share_gated():
         pl.when(level < 3)(lambda: send_gated(0, 1))
         pl.when(level > 0)(lambda: send_gated(0, -1))
+        pass_gated(0)
 
     def relay_gated(d):
         with scope(f"relay{d}"):
@@ -363,16 +369,13 @@
             def _():
                 took(gated_block(-d), ga_r.at[d - 1, 0])
                 pl.when(level < 3)(lambda: send_gated(d, 1))
+                pass_gated(-d)
 
             @pl.when(level + d < 4)
             def _():
                 took(gated_block(d), ga_r.at[d - 1, 1])
                 pl.when(level > 0)(lambda: send_gated(d, -1))
-
-    def pass_gated(k):
-        for n in range(4):
-            block = ga.at[n * quarter + i % quarter]
-            remote(block, block, put.at[12], one_r.at[3], (mate(k), t)).start()
+                pass_gated(d)
 
     near = chunk(0)
     spread(near[1:])
@@ -403,8 +406,6 @@
     weight_grad(hid, 1, dwd)
     with scope("gated"):
         relay_gated(3)
-        for k in range(1, quarter):
-            pass_gated(k)
 
     with scope("ret"):
         took(ret.at[pl.ds(1, n_sp - 1)], one_r.at[1])

time: 74.2 us -> 74 us (level)
  no operation moved by 1% of the time
where the time goes in v4:
time: 74 us; the launch traced here: 73.8 us
  Pallas kernels  73.2 us (99%)
    pallas_call x1, Pallas kernels, local(): pl.pallas_call(functools.partial(kernel, n_sp, n_tp), out_shape=[jax.Shap...  70.1 us
    pallas_call x1, Pallas kernels, local(): pl.pallas_call(functools.partial(settle, count), out_shape=[jax.ShapeDtyp...  3.05 us

profile of v4, /device:TPU:0, one launch (start us, length us, event | category | flops | bytes accessed | tf_op | source)
XLA Modules:
  0.0 73.8 jit_solution(4463711942073355318)
XLA Ops:
  0.6 70.1 %shard_map.162 = (bf16[512,2048]{1,0:T(8,128)(2,1)S(1)}, bf16[512,2048]{1,0:T(8,128)(2,1)S(1)}, bf16[512,2048]{1,0:T(8,128)(2,1)S(1)}, f32[256,512]{1,0:T(8,128)...) custom-call(s32[2,128]{1,0:T(2,128)} %bitcast.11, f32[2,128]{1,0:T(2,128)} %bitcast.12, ...), custom_call_target="tpu_custom_call" | custom-call | tf_op jit(solution)/shard_map/pallas_call | solution.py:573
  70.8 3.1 %shard_map.163 = (bf16[512,2048]{1,0:T(8,128)(2,1)}, bf16[512,2048]{1,0:T(8,128)(2,1)}, bf16[512,2048]{1,0:T(8,128)(2,1)}, f32[256,512]{1,0:T(8,128)}, bf16[128,...) custom-call(bf16[512,2048]{1,0:T(8,128)(2,1)S(1)} %get-tuple-element.21.refs_0_, ...), custom_call_target="tpu_custom_call" | custom-call | tf_op jit(solution)/shard_map/pallas_call | solution.py:642
